TPU v7x, 32 devices: a whole 2x2x4 slice. The times are simulated.
32 devices in a mesh: st: 16 (over z, y, x), tp: 2 (over core).
Axes of the slice: x: 2, y: 2, z: 4, core: 2. Of those that a mesh axis runs over, the one named last changes fastest.
Arguments:
- tokens: bfloat16 [4096, 2048], P('st'), may hold values from -6 to 6
- store: bfloat16 [64, 64, 2048], P('st'), may hold values from -6 to 6
- passage_ids: int32 [64, 4], P('st'), may hold values from 0 to 63, as said below
- w_query: bfloat16 [2048, 2048], P(None, 'tp'), may hold values from -0.125 to 0.125
- w_key: bfloat16 [2048, 512], P(None, 'tp'), may hold values from -0.125 to 0.125
- w_value: bfloat16 [2048, 512], P(None, 'tp'), may hold values from -0.125 to 0.125
- w_ret_query: bfloat16 [2048, 1024], P(None, 'tp'), may hold values from -0.125 to 0.125
- w_ret_key: bfloat16 [2048, 1024], P(None, 'tp'), may hold values from -0.125 to 0.125
- w_ret_value: bfloat16 [2048, 2048], P(None, 'tp'), may hold values from -0.125 to 0.125
- ret_rate: float32 [8], P('tp'), may hold values from 0.003 to 0.03
- ret_gain: float32 [2048], P('tp'), may hold values from 0.1 to 1.9
- gate_logit: float32 [2048], P('tp'), may hold values from -2 to 2
- out_grad: bfloat16 [4096, 2048], P('st', 'tp'), may hold values from -6 to 6
Outputs:
- grad_tokens: bfloat16 [4096, 2048], P(('st', 'tp'))
- grad_store: bfloat16 [64, 64, 2048], P(('st', 'tp'))
- grad_key_weight: float32 [2048, 512], P(None, 'tp')
Inputs may be any that keep to these rules, and one draw needn't show every extreme that they name: `passage_ids`: passage p lies on index p // 4 of st. The rows of one device name exactly 1 passage of every owner, so the 4 passages of a block differ.
All inputs are finite; a program needn't handle non-finite values.
Results may differ from a plain program's by a relative error of at most 0.012.
Values may be sent and summed in bfloat16 or wider, within the bound.
A program may use at most 192 MiB of HBM per device.

v0:
```python
import jax
import jax.numpy as jnp
from jax import lax
from jax.sharding import PartitionSpec as P

HEAD = 256
BLK = 64
KP = 4
MOST = 1
EPSILON = 1.0


def retention_grads(query_rows, key_rows, value_rows, rates, gains, cotangent):
    length = query_rows.shape[0]
    heads = rates.shape[0]
    queries = query_rows.reshape(length, heads, -1)
    keyset = key_rows.reshape(length, heads, -1)
    values = value_rows.reshape(length, heads, -1)
    positions = jnp.arange(length, dtype=jnp.float32)
    distance = positions[:, None] - positions[None, :]
    damping = jnp.where(
        distance >= 0.0, jnp.exp(-rates[:, None, None] * jnp.maximum(distance, 0.0)), 0.0
    ) * queries.shape[-1] ** (-0.5)
    raw = jnp.einsum("thd,shd->hts", queries, keyset, preferred_element_type=jnp.float32)
    weights = (raw * damping).astype(jnp.bfloat16)
    mixed = jnp.einsum("hts,she->the", weights, values, preferred_element_type=jnp.float32)
    inverse = lax.rsqrt(jnp.mean(mixed * mixed, axis=-1, keepdims=True) + EPSILON)
    scaled = cotangent.astype(jnp.float32).reshape(length, heads, -1) * gains.reshape(heads, -1)
    inner = jnp.mean(scaled * mixed, axis=-1, keepdims=True)
    grad_mixed = (inverse * scaled - inverse * inverse * inverse * mixed * inner).astype(
        jnp.bfloat16
    )
    grad_weights = (
        jnp.einsum("the,she->hts", grad_mixed, values, preferred_element_type=jnp.float32) * damping
    ).astype(jnp.bfloat16)
    grad_first = (
        jnp.einsum("hts,shd->thd", grad_weights, keyset, preferred_element_type=jnp.float32)
        .astype(jnp.bfloat16)
        .reshape(length, -1)
    )
    grad_second = (
        jnp.einsum("hts,thd->shd", grad_weights, queries, preferred_element_type=jnp.float32)
        .astype(jnp.bfloat16)
        .reshape(length, -1)
    )
    grad_third = (
        jnp.einsum("hts,the->she", weights, grad_mixed, preferred_element_type=jnp.float32)
        .astype(jnp.bfloat16)
        .reshape(length, -1)
    )
    return (grad_first, grad_second, grad_third)


def against_rows(left, weight):
    return lax.dot_general(
        left, weight, (((1,), (1,)), ((), ())), preferred_element_type=jnp.float32
    )


def across_rows(left, right):
    return lax.dot_general(
        left, right, (((0,), (0,)), ((), ())), preferred_element_type=jnp.float32
    )


def per_device(
    tokens,
    store,
    passage_ids,
    w_query,
    w_key,
    w_value,
    w_ret_query,
    w_ret_key,
    w_ret_value,
    ret_rate,
    ret_gain,
    gate_logit,
    out_grad,
):
    owners = lax.axis_size("st")
    pass_dev, plen, width = store.shape
    length = tokens.shape[0]
    kv_width = w_key.shape[1]
    kv_local = kv_width // HEAD
    group = w_query.shape[1] // HEAD // kv_local
    blocks = length // BLK
    slot_ids = passage_ids.reshape(-1)
    slot_count = slot_ids.shape[0]
    slot_owner = slot_ids // pass_dev
    slot_local = slot_ids % pass_dev
    order = jnp.arange(slot_count, dtype=jnp.int32)
    same_owner = slot_owner[:, None] == slot_owner[None, :]
    rank = jnp.sum(same_owner & (order[None, :] < order[:, None]), axis=1)
    position = slot_owner * MOST + rank
    cells = owners * MOST
    placed = jnp.arange(cells, dtype=jnp.int32)[:, None] == position[None, :]
    request = (jnp.sum(jnp.where(placed, slot_local[None, :] + 1, 0), axis=1) - 1).reshape(
        owners, MOST
    )
    incoming = lax.all_to_all(request, "st", split_axis=0, concat_axis=0, tiled=True)
    wanted = incoming.reshape(-1)
    valid = wanted >= 0
    safe = jnp.maximum(wanted, 0)
    placed_bf = placed.astype(jnp.bfloat16)
    store_rows = store.reshape(-1, width)
    nothing = jnp.zeros((), jnp.bfloat16)
    own_kv = jnp.concatenate(
        [
            jnp.dot(store_rows, w_key, preferred_element_type=jnp.float32).astype(jnp.bfloat16),
            jnp.dot(store_rows, w_value, preferred_element_type=jnp.float32).astype(jnp.bfloat16),
        ],
        axis=1,
    ).reshape(pass_dev, plen, 2 * kv_width)
    reply = jnp.where(valid[:, None, None], own_kv[safe], nothing).reshape(
        owners, MOST, plen, 2 * kv_width
    )
    arrived = lax.all_to_all(reply, "st", split_axis=0, concat_axis=0, tiled=True)
    slot_kv = (
        across_rows(placed_bf, arrived.reshape(cells, -1))
        .astype(jnp.bfloat16)
        .reshape(slot_count, plen, 2 * kv_width)
    )
    factor = HEAD ** (-0.5)
    gate = jax.nn.sigmoid(gate_logit)
    query_bf = jnp.dot(tokens, w_query, preferred_element_type=jnp.float32).astype(jnp.bfloat16)
    queries = query_bf.reshape(blocks, BLK, kv_local, group, HEAD)
    keys = slot_kv[:, :, :kv_width].reshape(blocks, KP * plen, kv_local, HEAD)
    values = slot_kv[:, :, kv_width:].reshape(blocks, KP * plen, kv_local, HEAD)
    scores = (
        jnp.einsum("btkgd,bskd->bkgts", queries, keys, preferred_element_type=jnp.float32) * factor
    )
    expo = jnp.exp(scores)
    probs = expo / jnp.sum(expo, axis=-1, keepdims=True)
    probs_bf = probs.astype(jnp.bfloat16)
    attn = jnp.einsum("bkgts,bskd->btkgd", probs_bf, values, preferred_element_type=jnp.float32)
    grad_attn = out_grad.astype(jnp.float32).reshape(
        blocks, BLK, kv_local, group, HEAD
    ) * gate.reshape(kv_local, group, HEAD)
    grad_attn_bf = grad_attn.astype(jnp.bfloat16)
    grad_probs = jnp.einsum(
        "btkgd,bskd->bkgts", grad_attn_bf, values, preferred_element_type=jnp.float32
    )
    delta = jnp.moveaxis(jnp.sum(grad_attn * attn, axis=-1), 1, 3)
    grad_scores = (probs * (grad_probs - delta[..., None]) * factor).astype(jnp.bfloat16)
    grad_query = (
        jnp.einsum("bkgts,bskd->btkgd", grad_scores, keys, preferred_element_type=jnp.float32)
        .astype(jnp.bfloat16)
        .reshape(length, -1)
    )
    grad_keys = (
        jnp.einsum("bkgts,btkgd->bskd", grad_scores, queries, preferred_element_type=jnp.float32)
        .astype(jnp.bfloat16)
        .reshape(slot_count, plen, kv_width)
    )
    grad_values = (
        jnp.einsum("bkgts,btkgd->bskd", probs_bf, grad_attn_bf, preferred_element_type=jnp.float32)
        .astype(jnp.bfloat16)
        .reshape(slot_count, plen, kv_width)
    )
    slot_grad = jnp.concatenate([grad_keys, grad_values], axis=2)
    outgoing = (
        jnp.dot(placed_bf, slot_grad.reshape(slot_count, -1), preferred_element_type=jnp.float32)
        .astype(jnp.bfloat16)
        .reshape(owners, MOST, plen, 2 * kv_width)
    )
    returned = lax.all_to_all(outgoing, "st", split_axis=0, concat_axis=0, tiled=True)
    matched = (jnp.arange(pass_dev, dtype=jnp.int32)[:, None] == wanted[None, :]).astype(
        jnp.bfloat16
    )
    passage_grad = jnp.dot(
        matched, returned.reshape(cells, -1), preferred_element_type=jnp.float32
    ).reshape(pass_dev * plen, 2 * kv_width)
    key_grad = passage_grad[:, :kv_width]
    upper = key_grad.astype(jnp.bfloat16)
    lower = (key_grad - upper.astype(jnp.float32)).astype(jnp.bfloat16)
    key_term = across_rows(store_rows, upper) + across_rows(store_rows, lower)
    grad_key_weight = lax.psum(key_term, "st")
    passage_bf = passage_grad.astype(jnp.bfloat16)
    grad_store = lax.psum_scatter(
        (
            against_rows(passage_bf[:, :kv_width], w_key)
            + against_rows(passage_bf[:, kv_width:], w_value)
        ).astype(jnp.bfloat16),
        "tp",
        scatter_dimension=0,
        tiled=True,
    ).astype(jnp.float32)
    grad_store = grad_store.astype(jnp.bfloat16).reshape(-1, plen, width)
    ret_query = jnp.dot(tokens, w_ret_query, preferred_element_type=jnp.float32).astype(
        jnp.bfloat16
    )
    ret_key = jnp.dot(tokens, w_ret_key, preferred_element_type=jnp.float32).astype(jnp.bfloat16)
    ret_value = jnp.dot(tokens, w_ret_value, preferred_element_type=jnp.float32).astype(
        jnp.bfloat16
    )
    grad_rq, grad_rk, grad_rv = retention_grads(
        ret_query, ret_key, ret_value, ret_rate, ret_gain, out_grad
    )
    total = against_rows(grad_query, w_query)
    total = total + against_rows(grad_rq, w_ret_query)
    total = total + against_rows(grad_rk, w_ret_key)
    grad_tokens = lax.psum_scatter(
        (total + against_rows(grad_rv, w_ret_value)).astype(jnp.bfloat16),
        "tp",
        scatter_dimension=0,
        tiled=True,
    )
    return (grad_tokens, grad_store, grad_key_weight)


def solution(mesh):
    return jax.shard_map(
        per_device,
        mesh=mesh,
        in_specs=(
            P("st", None),
            P("st", None, None),
            P("st", None),
            P(None, "tp"),
            P(None, "tp"),
            P(None, "tp"),
            P(None, "tp"),
            P(None, "tp"),
            P(None, "tp"),
            P("tp"),
            P("tp"),
            P("tp"),
            P("st", "tp"),
        ),
        out_specs=(P(("st", "tp"), None), P(("st", "tp"), None, None), P(None, "tp")),
        check_vma=False,
    )
```

profile of v0, /device:TPU:0, one launch (start us, length us, event | category | flops | bytes accessed | tf_op | source)
XLA Modules:
  0.0 243.0 jit_solution(17686899952723807470)
XLA Ops:
  10.0 8.3 %all-to-all-start = ((s32[16,1,1]{2,1,0:T(1,128)}), s32[16,1,1]{2,1,0:T(1,128)S(1)}, u32[]{:S(2)}, u32[]{:S(2)}) async-start(s32[16,1,1]{2,1,0:T(1,128)} %copy.79), calls=%async_computation | async-start | bytes 16384 | tf_op jit(solution)/shard_map/all_to_all | solution.py:101
  18.3 2.1 convolution_convert_fusion.10
  22.9 2.7 %all-to-all-done = s32[16,1,1]{2,1,0:T(1,128)S(1)} async-done(((s32[16,1,1]{2,1,0:T(1,128)}), s32[16,1,1]{2,1,0:T(1,128)S(1)}, u32[]{:S(2)}, u32[]{:S(2)}) %all-to-all-start) | async-done | bytes 96 | tf_op jit(solution)/shard_map/all_to_all | solution.py:101
  26.2 1.6 gather_fusion
  28.2 2.4 fusion.18
  30.6 4.3 %all-to-all-start.1 = ((bf16[16,1,64,512]{3,2,1,0:T(8,128)(2,1)}), bf16[16,1,64,512]{3,2,1,0:T(8,128)(2,1)}, u32[]{:S(2)}, u32[]{:S(2)}) async-start(bf16[16,1,64,512]{3,2,1,0:T(8,128)(2,1)} %fusion.18), calls=%async_computation.1 | async-start | bytes 2097152 | tf_op jit(solution)/shard_map/all_to_all | solution.py:118
  34.9 2.2 copy.89
  37.2 2.5 %reshape.312 = f32[4,64,4,256]{3,2,1,0:T(4,128)} reshape(bf16[256,1024]{1,0:T(8,128)(2,1)} %param.25) | data formatting | bytes 1572864 | tf_op jit(solution)/shard_map/reshape | solution.py:137
  39.7 2.5 %reshape.313 = f32[4,64,1,4,256]{4,3,1,0,2:T(4,128)} reshape(bf16[256,1024]{1,0:T(8,128)(2,1)} %param.25) | data formatting | bytes 1572864 | tf_op jit(solution)/shard_map/reshape | solution.py:137
  42.2 1.9 convolution_convert_fusion.8
  45.0 3.3 %convolution_convert_fusion.9 = bf16[256,512]{1,0:T(8,128)(2,1)} fusion(bf16[256,2048]{1,0:T(8,128)(2,1)} %param.13, bf16[2048,512]{1,0:T(8,128)(2,1)} %param.20), kind=kOutput, calls=%fused_computation.40 | convolution fusion | flops 537001984 | bytes 3407872 | tf_op jit(solution)/shard_map/dot_general | solution.py:193
  49.4 4.6 %convolution_convert_fusion.5 = bf16[256,1024]{1,0:T(8,128)(2,1)} fusion(bf16[256,2048]{1,0:T(8,128)(2,1)} %param.13, bf16[2048,1024]{1,0:T(8,128)(2,1)} %param.16), kind=kOutput, calls=%fused_computation.33 | convolution fusion | flops 1074003968 | bytes 5767168 | tf_op jit(solution)/shard_map/dot_general | solution.py:126
  54.0 2.2 reshape.310
  57.0 1.7 all-to-all-done.1
  58.7 1.8 copy.105
  66.8 1.3 copy.109
  68.2 6.0 %all-to-all-start.2 = ((bf16[16,1,64,512]{3,2,1,0:T(8,128)(2,1)}), bf16[16,1,64,512]{3,2,1,0:T(8,128)(2,1)}, u32[]{:S(2)}, u32[]{:S(2)}) async-start(bf16[16,1,64,512]{3,2,1,0:T(8,128)(2,1)} %bitcast.183), calls=%async_computation.3 | async-start | bytes 2097152 | tf_op jit(solution)/shard_map/all_to_all | solution.py:167
  74.4 1.5 fusion.10
  75.9 4.0 %convolution_convert_fusion.4 = bf16[256,1024]{1,0:T(8,128)(2,1)S(1)} fusion(bf16[256,2048]{1,0:T(8,128)(2,1)} %param.13, bf16[2048,1024]{1,0:T(8,128)(2,1)} %param.21), kind=kOutput, calls=%fused_computation.32 | convolution fusion | flops 1074003968 | bytes 5767168 | tf_op jit(solution)/shard_map/dot_general | solution.py:194
  83.6 13.5 %all-to-all-done.2 = bf16[16,1,64,512]{3,2,1,0:T(8,128)(2,1)} async-done(((bf16[16,1,64,512]{3,2,1,0:T(8,128)(2,1)}), bf16[16,1,64,512]{3,2,1,0:T(8,128)(2,1)}, u32[]{:S(2)}, u32[]{:S(2)}) %all-to-all-start.2) | async-done | bytes 1048608 | tf_op jit(solution)/shard_map/all_to_all | solution.py:167
  97.2 1.8 copy.110
  100.1 2.2 reshape.329
  102.3 1.5 fusion.36
  103.8 1.8 fusion.1
  105.6 1.4 convolution_convert_fusion.7
  107.4 3.7 %fusion.49 = f32[256,2048]{1,0:T(8,128)S(1)} fusion(bf16[256,1024]{0,1:T(8,128)(2,1)S(1)} %bitcast.195, bf16[2048,1024]{1,0:T(8,128)(2,1)} %param.21), kind=kOutput, calls=%fused_computation.101 | convolution fusion | flops 1073741824 | bytes 6815744 | tf_op jit(solution)/shard_map/dot_general | solution.py:55
  111.9 1.3 fusion.48
  114.8 1.7 fusion.2
  116.7 1.8 fusion.34
  118.5 1.5 fusion.3
  120.0 112.7 %all-reduce.2.cloned.1.call-done = f32[2048,256]{0,1:T(8,128)} async-done(((f32[2048,256]{0,1:T(8,128)}), f32[2048,256]{0,1:T(8,128)}) %all-reduce.2.cloned.1.call-update) | async-done | bytes 2097168 | tf_op jit(solution)/shard_map/psum | solution.py:178
  232.7 2.9 %copy.96 = f32[2048,256]{1,0:T(8,128)} copy(f32[2048,256]{0,1:T(8,128)} %all-reduce.2.cloned.1.call-done) | data formatting | bytes 4194304
  (106 shorter events, 22.3 us)
Async XLA Ops:
  8.0 34.2 %copy-start = (bf16[2048,512]{1,0:T(8,128)(2,1)S(1)}, bf16[2048,512]{1,0:T(8,128)(2,1)}, u32[]{:S(2)}) copy-start(bf16[2048,512]{1,0:T(8,128)(2,1)} %param.19) | copy-start | bytes 6291460
  8.0 12.5 %copy-start.1 = (bf16[4,64,2048]{2,1,0:T(8,128)(2,1)S(1)}, bf16[4,64,2048]{2,1,0:T(8,128)(2,1)}, u32[]{:S(2)}) copy-start(bf16[4,64,2048]{2,1,0:T(8,128)(2,1)} %param.14) | copy-start | bytes 3145732
  10.0 15.6 %all-to-all-start = ((s32[16,1,1]{2,1,0:T(1,128)}), s32[16,1,1]{2,1,0:T(1,128)S(1)}, u32[]{:S(2)}, u32[]{:S(2)}) async-start(s32[16,1,1]{2,1,0:T(1,128)} %copy.79), calls=%async_computation | async-start | bytes 16384 | tf_op jit(solution)/shard_map/all_to_all | solution.py:101
  18.3 2.2 copy-start.8
  30.6 28.1 %all-to-all-start.1 = ((bf16[16,1,64,512]{3,2,1,0:T(8,128)(2,1)}), bf16[16,1,64,512]{3,2,1,0:T(8,128)(2,1)}, u32[]{:S(2)}, u32[]{:S(2)}) async-start(bf16[16,1,64,512]{3,2,1,0:T(8,128)(2,1)} %fusion.18), calls=%async_computation.1 | async-start | bytes 2097152 | tf_op jit(solution)/shard_map/all_to_all | solution.py:118
  34.9 7.3 %copy-start.26 = (f32[4]{0:T(128)S(1)}, f32[4]{0:T(128)}, u32[]{:S(2)}) copy-start(f32[4]{0:T(128)} %param.22) | copy-start | bytes 52
  34.9 7.2 %copy-start.23 = (f32[1024]{0:T(1024)S(1)}, f32[1024]{0:T(1024)}, u32[]{:S(2)}) copy-start(f32[1024]{0:T(1024)} %param.23) | copy-start | bytes 12292
  34.9 7.2 %copy-start.24 = (f32[1024]{0:T(1024)S(1)}, f32[1024]{0:T(1024)}, u32[]{:S(2)}) copy-start(f32[1024]{0:T(1024)} %param.24) | copy-start | bytes 12292
  61.0 1.2 copy-start.3
  61.3 1.5 copy-start.18
  61.4 0.8 copy-start.4
  62.8 1.2 copy-start.19
  64.9 0.8 copy-start.10
  68.2 29.0 %all-to-all-start.2 = ((bf16[16,1,64,512]{3,2,1,0:T(8,128)(2,1)}), bf16[16,1,64,512]{3,2,1,0:T(8,128)(2,1)}, u32[]{:S(2)}, u32[]{:S(2)}) async-start(bf16[16,1,64,512]{3,2,1,0:T(8,128)(2,1)} %bitcast.183), calls=%async_computation.3 | async-start | bytes 2097152 | tf_op jit(solution)/shard_map/all_to_all | solution.py:167
  74.1 158.6 %all-reduce.2.cloned.1.call-start = ((), (), s32[]{:S(2)}) async-start(), calls=%async_computation.7 | async-start | bytes 4194304 | tf_op jit(solution)/shard_map/psum | solution.py:178
  75.9 4.0 %copy-start.14 = (bf16[4,256,256]{2,1,0:T(8,128)(2,1)}, bf16[4,256,256]{2,1,0:T(8,128)(2,1)S(1)}, u32[]{:S(2)}) copy-start(bf16[4,256,256]{2,1,0:T(8,128)(2,1)S(1)} %fusion.10) | copy-start | bytes 1572868
  75.9 4.0 %copy-start.2 = (f32[256,1024]{0,1:T(8,128)S(1)}, f32[256,1024]{0,1:T(8,128)}, u32[]{:S(2)}) copy-start(f32[256,1024]{0,1:T(8,128)} %copy.89) | copy-start | bytes 3145732
  80.3 1.1 copy-start.22
  81.4 1.3 copy-start.20
  81.9 0.8 copy-start.16
  102.3 1.5 copy-start.6
  105.5 1.5 copy-start.13
  105.5 1.5 copy-start.15
  105.6 130.0 %reduce-scatter.3.cloned.1.call-start = ((), (), s32[]{:S(2)}) async-start(), calls=%async_computation.5 | async-start | bytes 1572864 | tf_op jit(solution)/shard_map/reduce_scatter | solution.py:203
  107.4 3.7 %copy-start.5 = (bf16[16,64,256]{2,1,0:T(8,128)(2,1)S(1)}, bf16[16,64,256]{2,1,0:T(8,128)(2,1)}, u32[]{:S(2)}) copy-start(bf16[16,64,256]{2,1,0:T(8,128)(2,1)} %copy-done.4) | copy-start | bytes 1572868
  107.4 3.7 %copy-start.11 = (bf16[4,4,64,256]{3,2,1,0:T(8,128)(2,1)S(1)}, bf16[4,4,64,256]{3,2,1,0:T(8,128)(2,1)}, u32[]{:S(2)}) copy-start(bf16[4,4,64,256]{3,2,1,0:T(8,128)(2,1)} %copy-done.10) | copy-start | bytes 1572868
  107.4 4.5 %copy-start.25 = (bf16[2048,1024]{1,0:T(8,128)(2,1)S(1)}, bf16[2048,1024]{1,0:T(8,128)(2,1)}, u32[]{:S(2)}) copy-start(bf16[2048,1024]{1,0:T(8,128)(2,1)} %param.16) | copy-start | bytes 12582916
  113.2 1.6 copy-start.17
  113.3 1.6 copy-start.21
  114.8 1.8 copy-start.7
  116.6 119.0 %reduce-scatter.5.cloned.1.call-start = ((), (), s32[]{:S(2)}) async-start(), calls=%async_computation.6 | async-start | bytes 1572864 | tf_op jit(solution)/shard_map/reduce_scatter | solution.py:180
  116.7 1.8 copy-start.9
  (1 other events, 0.8 us)
Sparse Core Ops, SparseCore 0:
  105.7 126.9 all-reduce.1
Sparse Core Ops, SparseCore 1:
  116.7 8.7 reduce-scatter.2
  128.1 9.5 reduce-scatter.4
where the time goes:
time: 244 us; the launch traced here: 243 us
  waiting for transfers between devices  131 us (54%)
  matrix products  40.1 us (16%)
  local copies, waits for them, and re-layouts  31.6 us (13%)
  starting transfers between devices  19 us (8%)
  between operations  16 us (7%)
  other arithmetic  5.71 us (2%)
    psum x1, waiting for transfers between devices, per_device(): grad_key_weight = lax.psum(key_term, 'st')  113 us
    all_to_all x1, waiting for transfers between devices, per_device(): lax.all_to_all(outgoing, 'st', split_axis=0, concat_axis=0, tiled=True)  13.5 us
    unnamed x61, local copies, waits for them, and re-layouts  13.2 us
    dot_general x6, matrix products, against_rows(): lax.dot_general(left, weight, (((1,), (1,)), ((), ())), preferred_element...  10.7 us
    all_to_all x1, starting transfers between devices, per_device(): lax.all_to_all(request, 'st', split_axis=0, concat_axis=0, tiled=True)  8.34 us
    all_to_all x1, starting transfers between devices, per_device(): lax.all_to_all(outgoing, 'st', split_axis=0, concat_axis=0, tiled=True)  5.96 us
    reshape x2, local copies, waits for them, and re-layouts, per_device(): out_grad.astype(jnp.float32).reshape(blocks, BLK, kv_local, group, HEAD)  4.98 us
  transfers between devices with their start and end apart: 6, of which 4 were waited for; matrix products, arithmetic and copies ran while one was open for 21% of the time, Pallas kernels for 0%

commit v1 on v0

--- a/solution.py
+++ b/solution.py
@@ -175,7 +175,11 @@
     upper = key_grad.astype(jnp.bfloat16)
     lower = (key_grad - upper.astype(jnp.float32)).astype(jnp.bfloat16)
     key_term = across_rows(store_rows, upper) + across_rows(store_rows, lower)
-    grad_key_weight = lax.psum(key_term, "st")
+    grad_key_weight = key_term
+    for hop in (1, 2, 4, 8):
+        grad_key_weight = grad_key_weight + lax.ppermute(
+            grad_key_weight, "st", [(dev, dev ^ hop) for dev in range(16)]
+        )
     passage_bf = passage_grad.astype(jnp.bfloat16)
     grad_store = lax.psum_scatter(
         (

time: 244 us -> 356 us (1.46)
  waiting for transfers between devices: 131 us -> 230 us
  other arithmetic: 5.71 us -> 17 us
  starting transfers between devices: 19 us -> 29.3 us
  matrix products: 40.1 us -> 34.2 us
    ppermute x0 -> x4, waiting for transfers between devices: none -> 196 us  [per_device(): lax.ppermute(grad_key_weight, 'st', [(dev, dev ^ hop) for dev in range(16)])]
    psum x1 -> x0, waiting for transfers between devices: 113 us -> none  [per_device(): grad_key_weight = lax.psum(key_term, 'st')]
    add x0 -> x4, other arithmetic: none -> 12.1 us  [per_device(): grad_key_weight + lax.ppermute(grad_key_weight, 'st', [(dev, dev ^ hop) f...]
    ppermute x0 -> x4, starting transfers between devices: none -> 10.4 us  [per_device(): lax.ppermute(grad_key_weight, 'st', [(dev, dev ^ hop) for dev in range(16)])]
    all_to_all x1, waiting for transfers between devices: 1.66 us -> 12 us  [per_device(): lax.all_to_all(reply, 'st', split_axis=0, concat_axis=0, tiled=True)]
    all_to_all x1, waiting for transfers between devices: 13.5 us -> 20.2 us  [per_device(): lax.all_to_all(outgoing, 'st', split_axis=0, concat_axis=0, tiled=True)]
    unnamed x61 -> x53, local copies, waits for them, and re-layouts: 13.2 us -> 11.3 us
  transfers between devices with their start and end apart: 6 -> 9, of which waited for: 4 -> 7; matrix products, arithmetic and copies ran while one was open for 21% -> 14% of each run, Pallas kernels for 0% -> 0%
where the time goes in v1:
time: 356 us; the launch traced here: 355 us
  waiting for transfers between devices  230 us (65%)
  matrix products  34.2 us (10%)
  local copies, waits for them, and re-layouts  29.6 us (8%)
  starting transfers between devices  29.3 us (8%)
  other arithmetic  17 us (5%)
  between operations  14.6 us (4%)
    ppermute x4, waiting for transfers between devices, per_device(): lax.ppermute(grad_key_weight, 'st', [(dev, dev ^ hop) for dev in range(16)])  196 us
    all_to_all x1, waiting for transfers between devices, per_device(): lax.all_to_all(outgoing, 'st', split_axis=0, concat_axis=0, tiled=True)  20.2 us
    add x4, other arithmetic, per_device(): grad_key_weight + lax.ppermute(grad_key_weight, 'st', [(dev, dev ^ hop) f...  12.1 us
    all_to_all x1, waiting for transfers between devices, per_device(): lax.all_to_all(reply, 'st', split_axis=0, concat_axis=0, tiled=True)  12 us
    unnamed x53, local copies, waits for them, and re-layouts  11.3 us
    ppermute x4, starting transfers between devices, per_device(): lax.ppermute(grad_key_weight, 'st', [(dev, dev ^ hop) for dev in range(16)])  10.4 us
    all_to_all x1, starting transfers between devices, per_device(): lax.all_to_all(request, 'st', split_axis=0, concat_axis=0, tiled=True)  8.34 us
    dot_general x6, matrix products, against_rows(): lax.dot_general(left, weight, (((1,), (1,)), ((), ())), preferred_element...  8.27 us
  transfers between devices with their start and end apart: 9, of which 7 were waited for; matrix products, arithmetic and copies ran while one was open for 14% of the time, Pallas kernels for 0%

profile of v1, /device:TPU:0, one launch (start us, length us, event | category | flops | bytes accessed | tf_op | source)
XLA Modules:
  0.0 355.2 jit_solution(11450373126892977765)
XLA Ops:
  9.1 8.3 %all-to-all-start = ((s32[16,1,1]{2,1,0:T(1,128)}), s32[16,1,1]{2,1,0:T(1,128)S(1)}, u32[]{:S(2)}, u32[]{:S(2)}) async-start(s32[16,1,1]{2,1,0:T(1,128)} %copy.79), calls=%async_computation | async-start | bytes 16384 | tf_op jit(solution)/shard_map/all_to_all | solution.py:101
  17.5 2.1 convolution_convert_fusion.10
  22.0 2.7 all-to-all-done
  27.4 2.3 fusion.18
  29.7 4.4 %all-to-all-start.1 = ((bf16[16,1,64,512]{3,2,1,0:T(8,128)(2,1)}), bf16[16,1,64,512]{3,2,1,0:T(8,128)(2,1)}, u32[]{:S(2)}, u32[]{:S(2)}) async-start(bf16[16,1,64,512]{3,2,1,0:T(8,128)(2,1)} %fusion.18), calls=%async_computation.1 | async-start | bytes 2097152 | tf_op jit(solution)/shard_map/all_to_all | solution.py:118
  34.1 2.5 reshape.312
  36.6 2.5 reshape.313
  39.1 4.6 %convolution_convert_fusion.5 = bf16[256,1024]{1,0:T(8,128)(2,1)} fusion(bf16[256,2048]{1,0:T(8,128)(2,1)} %param.13, bf16[2048,1024]{1,0:T(8,128)(2,1)} %param.16), kind=kOutput, calls=%fused_computation.33 | convolution fusion | flops 1074003968 | bytes 5767168 | tf_op jit(solution)/shard_map/dot_general | solution.py:126
  43.6 2.2 reshape.310
  45.9 12.0 %all-to-all-done.1 = bf16[16,1,64,512]{3,2,1,0:T(8,128)(2,1)} async-done(((bf16[16,1,64,512]{3,2,1,0:T(8,128)(2,1)}), bf16[16,1,64,512]{3,2,1,0:T(8,128)(2,1)}, u32[]{:S(2)}, u32[]{:S(2)}) %all-to-all-start.1) | async-done | bytes 1048608 | tf_op jit(solution)/shard_map/all_to_all | solution.py:118
  57.8 1.8 copy.105
  67.3 6.0 %all-to-all-start.2 = ((bf16[16,1,64,512]{3,2,1,0:T(8,128)(2,1)}), bf16[16,1,64,512]{3,2,1,0:T(8,128)(2,1)}, u32[]{:S(2)}, u32[]{:S(2)}) async-start(bf16[16,1,64,512]{3,2,1,0:T(8,128)(2,1)} %bitcast.183), calls=%async_computation.3 | async-start | bytes 2097152 | tf_op jit(solution)/shard_map/all_to_all | solution.py:167
  73.5 2.6 convolution_convert_fusion.8
  76.1 20.2 %all-to-all-done.2 = bf16[16,1,64,512]{3,2,1,0:T(8,128)(2,1)} async-done(((bf16[16,1,64,512]{3,2,1,0:T(8,128)(2,1)}), bf16[16,1,64,512]{3,2,1,0:T(8,128)(2,1)}, u32[]{:S(2)}, u32[]{:S(2)}) %all-to-all-start.2) | async-done | bytes 1048608 | tf_op jit(solution)/shard_map/all_to_all | solution.py:167
  96.3 1.8 copy.110
  99.2 2.2 reshape.329
  102.9 1.8 fusion.1
  109.3 1.8 copy.102
  112.7 3.5 convolution_convert_fusion.4
  117.5 32.5 %collective-permute-done = f32[2048,256]{0,1:T(8,128)} collective-permute-done((f32[2048,256]{0,1:T(8,128)}, f32[2048,256]{0,1:T(8,128)}, u32[]{:S(2)}, u32[]{:S(2)}) %collective-permute-start) | collective-permute-done | bytes 2097184 | tf_op jit(solution)/shard_map/ppermute | solution.py:180
  149.9 2.7 add.111
  152.6 2.4 collective-permute-start.1
  160.6 37.2 %collective-permute-done.1 = f32[2048,256]{0,1:T(8,128)S(1)} collective-permute-done((f32[2048,256]{0,1:T(8,128)S(1)}, f32[2048,256]{0,1:T(8,128)S(1)}, u32[]{:S(2)}, u32[]{:S(2)}) %collective-permute-start.1) | collective-permute-done | bytes 2097184 | tf_op jit(solution)/shard_map/ppermute | solution.py:180
  199.5 4.4 %collective-permute-start.2 = (f32[2048,256]{0,1:T(8,128)}, f32[2048,256]{0,1:T(8,128)}, u32[]{:S(2)}, u32[]{:S(2)}) collective-permute-start(f32[2048,256]{0,1:T(8,128)} %add.112), channel_id=1, source_target_pairs={{0,8},{2,10},{4,12},{6,14},{8,0},{10,2},{12,4},{14,6},{16,24},{18,... | collective-permute-start | bytes 6291464 | tf_op jit(solution)/shard_map/ppermute | solution.py:180
  203.8 1.7 fusion.2
  205.7 1.7 fusion.34
  207.4 39.9 %collective-permute-done.2 = f32[2048,256]{0,1:T(8,128)} collective-permute-done((f32[2048,256]{0,1:T(8,128)}, f32[2048,256]{0,1:T(8,128)}, u32[]{:S(2)}, u32[]{:S(2)}) %collective-permute-start.2) | collective-permute-done | bytes 2097184 | tf_op jit(solution)/shard_map/ppermute | solution.py:180
  247.3 3.9 %add.113 = f32[2048,256]{0,1:T(8,128)} add(f32[2048,256]{0,1:T(8,128)} %add.112, f32[2048,256]{0,1:T(8,128)} %collective-permute-done.2) | non-fusion elementwise | flops 524288 | bytes 6291456 | tf_op jit(solution)/shard_map/add | solution.py:180
  251.1 2.9 collective-permute-start.3
  255.6 86.1 %collective-permute-done.3 = f32[2048,256]{0,1:T(8,128)} collective-permute-done((f32[2048,256]{0,1:T(8,128)}, f32[2048,256]{0,1:T(8,128)}, u32[]{:S(2)}, u32[]{:S(2)}) %collective-permute-start.3) | collective-permute-done | bytes 2097184 | tf_op jit(solution)/shard_map/ppermute | solution.py:180
  341.6 3.9 %add.114 = f32[2048,256]{0,1:T(8,128)} add(f32[2048,256]{0,1:T(8,128)} %add.113, f32[2048,256]{0,1:T(8,128)} %collective-permute-done.3) | non-fusion elementwise | flops 524288 | bytes 6291456 | tf_op jit(solution)/shard_map/add | solution.py:180
  345.5 2.9 copy.96
  (107 shorter events, 33.3 us)
Async XLA Ops:
  7.2 66.3 %copy-start = (bf16[2048,512]{1,0:T(8,128)(2,1)S(1)}, bf16[2048,512]{1,0:T(8,128)(2,1)}, u32[]{:S(2)}) copy-start(bf16[2048,512]{1,0:T(8,128)(2,1)} %param.19) | copy-start | bytes 6291460
  7.2 12.5 %copy-start.1 = (bf16[4,64,2048]{2,1,0:T(8,128)(2,1)S(1)}, bf16[4,64,2048]{2,1,0:T(8,128)(2,1)}, u32[]{:S(2)}) copy-start(bf16[4,64,2048]{2,1,0:T(8,128)(2,1)} %param.14) | copy-start | bytes 3145732
  9.1 15.6 %all-to-all-start = ((s32[16,1,1]{2,1,0:T(1,128)}), s32[16,1,1]{2,1,0:T(1,128)S(1)}, u32[]{:S(2)}, u32[]{:S(2)}) async-start(s32[16,1,1]{2,1,0:T(1,128)} %copy.79), calls=%async_computation | async-start | bytes 16384 | tf_op jit(solution)/shard_map/all_to_all | solution.py:101
  17.5 2.2 copy-start.7
  29.7 28.1 %all-to-all-start.1 = ((bf16[16,1,64,512]{3,2,1,0:T(8,128)(2,1)}), bf16[16,1,64,512]{3,2,1,0:T(8,128)(2,1)}, u32[]{:S(2)}, u32[]{:S(2)}) async-start(bf16[16,1,64,512]{3,2,1,0:T(8,128)(2,1)} %fusion.18), calls=%async_computation.1 | async-start | bytes 2097152 | tf_op jit(solution)/shard_map/all_to_all | solution.py:118
  34.1 5.0 %copy-start.16 = (f32[1024]{0:T(1024)S(1)}, f32[1024]{0:T(1024)}, u32[]{:S(2)}) copy-start(f32[1024]{0:T(1024)} %param.24) | copy-start | bytes 12292
  60.1 1.2 copy-start.2
  60.5 1.5 copy-start.13
  60.6 0.8 copy-start.3
  61.9 1.2 copy-start.14
  64.1 0.8 copy-start.9
  67.3 29.0 %all-to-all-start.2 = ((bf16[16,1,64,512]{3,2,1,0:T(8,128)(2,1)}), bf16[16,1,64,512]{3,2,1,0:T(8,128)(2,1)}, u32[]{:S(2)}, u32[]{:S(2)}) async-start(bf16[16,1,64,512]{3,2,1,0:T(8,128)(2,1)} %bitcast.183), calls=%async_computation.3 | async-start | bytes 2097152 | tf_op jit(solution)/shard_map/all_to_all | solution.py:167
  73.2 275.2 %reduce-scatter.3.cloned.1.call-start = ((), (), s32[]{:S(2)}) async-start(), calls=%async_computation.5 | async-start | bytes 1572864 | tf_op jit(solution)/shard_map/reduce_scatter | solution.py:207
  101.4 1.5 copy-start.5
  102.9 2.5 copy-start.11
  102.9 2.6 copy-start.20
  104.7 3.5 copy-start.22
  104.7 3.5 copy-start.17
  104.7 45.3 %collective-permute-start = (f32[2048,256]{0,1:T(8,128)}, f32[2048,256]{0,1:T(8,128)}, u32[]{:S(2)}, u32[]{:S(2)}) collective-permute-start(f32[2048,256]{0,1:T(8,128)} %fusion.1), channel_id=1, source_target_pairs={{0,2},{2,0},{4,6},{6,4},{8,10},{10,8},{12,14},{14,12},{16,18},{18,... | collective-permute-start | bytes 6291464 | tf_op jit(solution)/shard_map/ppermute | solution.py:180
  111.1 1.6 copy-start.21
  117.4 37.9 %copy-start.15 = (bf16[256,512]{0,1:T(8,128)(2,1)S(1)}, bf16[256,512]{0,1:T(8,128)(2,1)}, u32[]{:S(2)}) copy-start(bf16[256,512]{0,1:T(8,128)(2,1)} %copy.102) | copy-start | bytes 786436
  149.9 6.0 %copy-start.18 = (bf16[2048,1024]{1,0:T(8,128)(2,1)S(1)}, bf16[2048,1024]{1,0:T(8,128)(2,1)}, u32[]{:S(2)}) copy-start(bf16[2048,1024]{1,0:T(8,128)(2,1)} %param.21) | copy-start | bytes 12582916
  152.6 45.2 %collective-permute-start.1 = (f32[2048,256]{0,1:T(8,128)S(1)}, f32[2048,256]{0,1:T(8,128)S(1)}, u32[]{:S(2)}, u32[]{:S(2)}) collective-permute-start(f32[2048,256]{0,1:T(8,128)S(1)} %add.111), channel_id=1, source_target_pairs={{0,4},{2,6},{4,0},{6,2},{8,12},{10,14},{12,8},{14,10},{16,20},{18,... | collective-permute-start | bytes 6291464 | tf_op jit(solution)/shard_map/ppermute | solution.py:180
  156.0 1.3 copy-start.4
  156.0 1.3 copy-start.10
  156.0 2.5 copy-start.19
  160.6 43.2 %copy-start.12 = (bf16[2048,512]{1,0:T(8,128)(2,1)S(1)}, bf16[2048,512]{1,0:T(8,128)(2,1)}, u32[]{:S(2)}) copy-start(bf16[2048,512]{1,0:T(8,128)(2,1)} %param.20) | copy-start | bytes 6291460
  199.5 47.8 %collective-permute-start.2 = (f32[2048,256]{0,1:T(8,128)}, f32[2048,256]{0,1:T(8,128)}, u32[]{:S(2)}, u32[]{:S(2)}) collective-permute-start(f32[2048,256]{0,1:T(8,128)} %add.112), channel_id=1, source_target_pairs={{0,8},{2,10},{4,12},{6,14},{8,0},{10,2},{12,4},{14,6},{16,24},{18,... | collective-permute-start | bytes 6291464 | tf_op jit(solution)/shard_map/ppermute | solution.py:180
  203.8 1.8 copy-start.6
  205.6 142.8 %reduce-scatter.5.cloned.1.call-start = ((), (), s32[]{:S(2)}) async-start(), calls=%async_computation.6 | async-start | bytes 1572864 | tf_op jit(solution)/shard_map/reduce_scatter | solution.py:184
  207.4 46.7 %copy-start.8 = (bf16[2048,256]{1,0:T(8,128)(2,1)S(1)}, bf16[2048,256]{1,0:T(8,128)(2,1)}, u32[]{:S(2)}) copy-start(bf16[2048,256]{1,0:T(8,128)(2,1)} %param.18) | copy-start | bytes 3145732
  251.1 90.5 %collective-permute-start.3 = (f32[2048,256]{0,1:T(8,128)}, f32[2048,256]{0,1:T(8,128)}, u32[]{:S(2)}, u32[]{:S(2)}) collective-permute-start(f32[2048,256]{0,1:T(8,128)} %add.113), channel_id=1, source_target_pairs={{0,16},{2,18},{4,20},{6,22},{8,24},{10,26},{12,28},{14,30},{16,0},... | collective-permute-start | bytes 6291464 | tf_op jit(solution)/shard_map/ppermute | solution.py:180
Sparse Core Ops, SparseCore 0:
  205.7 7.3 reduce-scatter.2
  255.7 6.3 reduce-scatter.4
